TPU v7x, 32 devices: a whole 2x2x4 slice. The times are simulated.
32 devices in a mesh: sp: 8 (over z, x), tp: 4 (over y, core).
Axes of the slice: x: 2, y: 2, z: 4, core: 2. Of those that a mesh axis runs over, the one named last changes fastest.
Arguments:
- queries: bfloat16 [2048, 1024], P('sp', 'tp'), may hold values from -6 to 6
- keys: bfloat16 [2048, 256], P('sp'), may hold values from -6 to 6
- values: bfloat16 [2048, 256], P('sp'), may hold values from -6 to 6
- sink: float32 [16], P('tp'), may hold values from 3 to 6
- w_out: bfloat16 [1024, 2048], P('tp'), may hold values from -0.1875 to 0.1875
- stream: bfloat16 [2048, 2048], P(('sp', 'tp')), may hold values from -6 to 6
- gain: bfloat16 [2048], replicated, may hold values from 0.099609375 to 1.8984375
- routes: int32 [2048, 4], P('sp'), may hold values from 0 to 63, all different within a row; in each aligned block of 64 rows (0 to 63, 64 to 127, ...) at most 8 rows name the same one
- route_weights: float32 [2048, 4], P('sp'), may hold values from 0.2 to 1
- w_gate: bfloat16 [64, 1024, 2048], P('sp', 'tp'), may hold values from -0.125 to 0.125
- w_up: bfloat16 [64, 1024, 2048], P('sp', 'tp'), may hold values from -0.125 to 0.125
- w_down: bfloat16 [64, 1024, 2048], P('sp', None, 'tp'), may hold values from -0.1875 to 0.1875
- shared_gate: bfloat16 [1024, 2048], P('tp'), may hold values from -0.125 to 0.125
- shared_up: bfloat16 [1024, 2048], P('tp'), may hold values from -0.125 to 0.125
- shared_down: bfloat16 [1024, 2048], P(None, 'tp'), may hold values from -0.1875 to 0.1875
Outputs:
- layer_out: bfloat16 [2048, 2048], P('sp', 'tp')
Inputs may be any that keep to these rules, and one draw needn't show every extreme that they name: `routes`: in each aligned block of 64 rows no expert is named in more than 8 rows, and some blocks reach 8; a row names 4 different experts.
All inputs are finite; a program needn't handle non-finite values.
Results may differ from a plain program's by a relative error of at most 0.014.
Values may be sent and summed in bfloat16 or wider, within the bound.
A program may use at most 128 MiB of HBM per device.

v0:
```python
import jax
import jax.numpy as jnp
from jax import lax
from jax.sharding import PartitionSpec as P

D = 2048
HEADS = 16
KV_HEADS = 4
HD = 64
WINDOW = 128
EXPERTS = 64
TOPK = 4


NORM_EPS = 1e-05


def with_halo(array, sides, width):
    for axis, dim in sides:
        devices, length = (lax.axis_size(axis), array.shape[dim])
        up = [(i, (i + 1) % devices) for i in range(devices - 1)]
        down = [(j, i) for i, j in up]
        last = lax.slice_in_dim(array, length - width, length, axis=dim)
        leading = lax.slice_in_dim(array, 0, width, axis=dim)
        before = lax.ppermute(last, axis, up)
        after = lax.ppermute(leading, axis, down)
        array = jnp.concatenate([before, array, after], axis=dim)
    return array


def slot_ids(block_routes, capacity):
    flat_routes = block_routes.reshape(-1)
    hit_table = (flat_routes[:, None] == jnp.arange(EXPERTS)[None, :]).astype(jnp.int32)
    earlier = jnp.cumsum(hit_table, axis=0) - hit_table
    slot_rank = jnp.sum(earlier * hit_table, axis=1)
    return flat_routes * capacity + slot_rank


def local(
    queries,
    keys,
    values,
    sink,
    w_out,
    stream,
    gain,
    routes,
    route_weights,
    w_gate,
    w_up,
    w_down,
    shared_gate,
    shared_up,
    shared_down,
):
    tok_dev = queries.shape[0]
    n_tp = lax.axis_size("tp")
    n_sp = lax.axis_size("sp")
    tp_idx = lax.axis_index("tp")
    sp_idx = lax.axis_index("sp")
    heads_dev = HEADS // n_tp
    group = HEADS // KV_HEADS
    kv_head = tp_idx * heads_dev // group
    key_own = lax.dynamic_slice_in_dim(keys, kv_head * HD, HD, 1)
    value_own = lax.dynamic_slice_in_dim(values, kv_head * HD, HD, 1)
    paired = jnp.concatenate([key_own, value_own], axis=1)
    padded = with_halo(paired, (("sp", 0),), WINDOW)
    blocks = tok_dev // WINDOW
    framed = padded.reshape(blocks + 2, WINDOW, 2 * HD)
    banded = jnp.concatenate([framed[:-2], framed[1:-1], framed[2:]], axis=1)
    key_band = banded[:, :, :HD]
    value_band = banded[:, :, HD:]
    query_blocks = queries.reshape(blocks, WINDOW, heads_dev, HD)
    scores = jnp.einsum(
        "nqhd,njd->nhqj", query_blocks, key_band, preferred_element_type=jnp.float32
    ) * HD ** (-0.5)
    offset = sp_idx * tok_dev
    seq_total = tok_dev * n_sp
    query_pos = (
        offset + jnp.arange(blocks)[:, None, None] * WINDOW + jnp.arange(WINDOW)[None, :, None]
    )
    key_pos = (
        offset
        - WINDOW
        + jnp.arange(blocks)[:, None, None] * WINDOW
        + jnp.arange(3 * WINDOW)[None, None, :]
    )
    allowed = (jnp.abs(query_pos - key_pos) <= WINDOW) & (key_pos >= 0) & (key_pos < seq_total)
    scores = jnp.where(allowed[:, None], scores, -jnp.inf)
    sink_level = sink.reshape(1, heads_dev, 1, 1)
    row_peak = jnp.maximum(scores.max(-1, keepdims=True), sink_level)
    probabilities = jnp.exp(scores - row_peak)
    denominator = probabilities.sum(-1, keepdims=True) + jnp.exp(sink_level - row_peak)
    weights = (probabilities / denominator).astype(jnp.bfloat16)
    attended = jnp.einsum("nhqj,njd->nqhd", weights, value_band, preferred_element_type=jnp.float32)
    attended = attended.astype(jnp.bfloat16).reshape(tok_dev, heads_dev * HD)
    rows_dev = tok_dev // n_tp
    d_dev = w_down.shape[2]
    projected = lax.psum_scatter(
        jnp.dot(attended, w_out, preferred_element_type=jnp.float32),
        "tp",
        scatter_dimension=0,
        tiled=True,
    )
    mixed_rows = (stream.astype(jnp.float32) + projected).astype(jnp.bfloat16)
    whole_rows = lax.all_gather(mixed_rows, "tp", axis=0, tiled=True)
    wide_rows = whole_rows.astype(jnp.float32)
    scale_rows = lax.rsqrt(jnp.mean(wide_rows * wide_rows, axis=-1, keepdims=True) + NORM_EPS)
    normed = (wide_rows * scale_rows * gain.astype(jnp.float32)).astype(jnp.bfloat16)
    residual = lax.dynamic_slice_in_dim(wide_rows, tp_idx * d_dev, d_dev, 1)
    exp_dev = w_gate.shape[0]
    capacity = max(1, 2 * tok_dev * TOPK // (n_tp * EXPERTS))
    slot_count = EXPERTS * capacity
    blocked_routes = routes.reshape(n_tp, rows_dev, TOPK)
    destination = jax.vmap(lambda block_routes: slot_ids(block_routes, capacity))(blocked_routes)
    slot_select = destination[:, None, :] == jnp.arange(slot_count)[None, :, None]
    slot_select = slot_select.reshape(n_tp, slot_count, rows_dev, TOPK).astype(jnp.float32)
    dispatch_table = jnp.sum(slot_select, axis=-1).astype(jnp.bfloat16)
    combine_table = jnp.sum(slot_select * route_weights.reshape(n_tp, 1, rows_dev, TOPK), axis=-1)
    normed_blocks = normed.reshape(n_tp, rows_dev, D)
    own_table = lax.dynamic_index_in_dim(dispatch_table, tp_idx, 0, keepdims=False)
    own_rows = lax.dynamic_index_in_dim(normed_blocks, tp_idx, 0, keepdims=False)
    outgoing = jnp.dot(own_table, own_rows, preferred_element_type=jnp.float32).astype(jnp.bfloat16)
    arrived = lax.all_to_all(outgoing, "sp", split_axis=0, concat_axis=0, tiled=True)
    arrived = arrived.reshape(1, n_sp, exp_dev, capacity, D)
    piece_rows = lax.all_gather(arrived, "tp", axis=0, tiled=True)
    gate_act = jnp.einsum(
        "tsecd,efd->tsecf", piece_rows, w_gate, preferred_element_type=jnp.float32
    )
    up_act = jnp.einsum("tsecd,efd->tsecf", piece_rows, w_up, preferred_element_type=jnp.float32)
    hidden = (jax.nn.silu(gate_act) * up_act).astype(jnp.bfloat16)
    shared_gate_act = jnp.einsum(
        "td,fd->tf", normed, shared_gate, preferred_element_type=jnp.float32
    )
    shared_up_act = jnp.einsum("td,fd->tf", normed, shared_up, preferred_element_type=jnp.float32)
    shared_hidden = (jax.nn.silu(shared_gate_act) * shared_up_act).astype(jnp.bfloat16)
    shared_hidden = shared_hidden.reshape(1, 1, 1, tok_dev, shared_hidden.shape[1])
    expert_piece = lax.all_gather(hidden, "tp", axis=4, tiled=True)
    shared_piece = lax.all_gather(shared_hidden, "tp", axis=4, tiled=True)
    piece_width = expert_piece.shape[4]
    routed_total = jnp.einsum(
        "tsecf,efd->tsecd", expert_piece, w_down, preferred_element_type=jnp.float32
    )
    shared_total = jnp.dot(
        shared_piece.reshape(tok_dev, piece_width), shared_down, preferred_element_type=jnp.float32
    )
    returned = lax.all_to_all(
        routed_total.astype(jnp.bfloat16), "sp", split_axis=1, concat_axis=1, tiled=True
    )
    returned = returned.reshape(n_tp, slot_count, d_dev).astype(jnp.float32)
    routed = jnp.einsum("tmr,tmd->trd", combine_table, returned, precision=lax.Precision.HIGHEST)
    routed = routed.reshape(tok_dev, d_dev)
    return (residual + routed + shared_total).astype(jnp.bfloat16)


def solution(mesh):
    placed = (
        P("sp", "tp"),
        P("sp", None),
        P("sp", None),
        P("tp"),
        P("tp", None),
        P(("sp", "tp"), None),
        P(),
        P("sp", None),
        P("sp", None),
        P("sp", "tp", None),
        P("sp", "tp", None),
        P("sp", None, "tp"),
        P("tp", None),
        P("tp", None),
        P(None, "tp"),
    )
    return jax.shard_map(
        local, mesh=mesh, in_specs=placed, out_specs=P("sp", "tp"), check_vma=False
    )
```

profile of v0, /device:TPU:0, one launch (start us, length us, event | category | flops | bytes accessed | tf_op | source)
XLA Modules:
  0.0 317.8 jit_solution(6857469026317906916)
XLA Ops:
  6.5 1.1 constant_dynamic-slice_fusion
  7.7 4.9 %collective-permute-start = (bf16[128,128]{1,0:T(8,128)(2,1)S(1)}, bf16[128,128]{1,0:T(8,128)(2,1)S(1)}, u32[]{:S(2)}, u32[]{:S(2)}) collective-permute-start(bf16[128,128]{1,0:T(8,128)(2,1)S(1)} %get-tuple-element.10), channel_id=1, source_target_pairs={{0,4},{4,8},{8,12},{12,16},{16,20},{20,24},{24,28},{1,5},{5,9},{9,... | collective-permute-start | bytes 98312 | tf_op jit(solution)/shard_map/ppermute | solution.py:25
  12.6 1.3 collective-permute-start.1
  14.2 0.5 fusion.19
  14.6 1.1 reshape.199
  15.7 2.7 collective-permute-done.1
  18.6 0.1 copy.54
  18.8 0.1 copy.53
  18.9 0.4 fusion.41
  19.5 0.2 fusion.14
  19.8 0.4 fusion.17
  20.2 0.1 copy.59
  20.4 1.8 fusion.27
  22.3 32.5 %reduce-scatter.2.cloned.1.call-done = f32[64,2048]{1,0:T(8,128)} async-done(((f32[256,2048]{1,0:T(8,128)}), f32[64,2048]{1,0:T(8,128)}) %reduce-scatter.2.cloned.1.call-update) | async-done | bytes 524304 | tf_op jit(solution)/shard_map/reduce_scatter | solution.py:99
  54.7 1.8 add_convert_fusion
  56.6 0.1 copy.61
  56.7 0.1 eq.39
  57.0 0.1 copy.60
  57.2 2.4 reduce-window.6
  59.7 0.1 copy.63
  59.9 0.2 fusion.22
  60.0 0.1 reduce_sum.49
  60.4 1.3 convert_reduce_fusion
  61.7 11.7 %all-gather.5.cloned.1.call-done = bf16[256,2048]{1,0:T(8,128)(2,1)} async-done(((bf16[64,2048]{1,0:T(8,128)(2,1)}), bf16[256,2048]{1,0:T(8,128)(2,1)}) %all-gather.5.cloned.1.call-update) | async-done | bytes 1048592 | tf_op jit(solution)/shard_map/all_gather | solution.py:106
  73.4 1.5 multiply_reduce_fusion
  74.9 1.5 multiply_convert_fusion
  76.5 0.7 convolution_convert_fusion
  77.2 53.9 %all_to_all.14 = bf16[8,64,2048]{2,1,0:T(8,128)(2,1)S(1)} all-to-all(bf16[8,64,2048]{2,1,0:T(8,128)(2,1)S(1)} %bitcast.114), channel_id=1, replica_groups=mesh['sp'=8,'tp'=4] {'sp'}, dimensions={0} | all-to-all | bytes 4194304 | tf_op jit(solution)/shard_map/all_to_all | solution.py:124
  131.1 1.5 copy.68
  132.6 0.2 all-gather.9.cloned.1.call-start
  132.8 56.3 %all-gather.7.cloned.1.call-done = bf16[4,8,8,8,2048]{4,3,1,0,2:T(8,128)(2,1)} async-done(((bf16[1,8,8,8,2048]{4,3,1,0,2:T(8,128)(2,1)}), bf16[4,8,8,8,2048]{4,3,1,0,2:T(8,128)(2,1)}) %all-gather.7.cloned.1.call-update) | async-done | bytes 8388624 | tf_op jit(solution)/shard_map/all_gather | solution.py:126
  189.2 8.1 %fusion.4 = f32[8,4,8,8,256]{4,3,2,1,0:T(8,128)S(1)} fusion(bf16[4,8,8,8,2048]{4,3,1,0,2:T(8,128)(2,1)} %all-gather.7.cloned.1.call-done, bf16[8,256,2048]{2,1,0:T(8,128)(2,1)} %param.24), kind=kOutput, calls=%fused_computation.4 | convolution fusion | flops 2147483648 | bytes 18874368 | tf_op jit(solution)/shard_map/tsecd,efd->tsecf/dot_general | solution.py:127
  197.3 11.4 %fusion.6 = bf16[4,8,8,8,256]{4,3,1,0,2:T(8,128)(2,1)} fusion(f32[8,4,8,8,256]{4,3,2,1,0:T(8,128)S(1)} %fusion.4, bf16[4,8,8,8,2048]{4,3,1,0,2:T(8,128)(2,1)} %all-gather.7.cloned.1.call-done, bf16[8,256,2048]{2,1,0:T(8,128)(2,1)} %param.25), kind=kOutput, calls=%fused_computation.8 | convolution fusion | flops 2150629376 | bytes 19922944 | tf_op jit(solution)/shard_map/tsecd,efd->tsecf/dot_general | solution.py:130
  208.7 35.2 %all-gather.9.cloned.1.call-done = bf16[4,8,8,8,1024]{4,3,1,0,2:T(8,128)(2,1)} async-done(((bf16[4,8,8,8,256]{4,3,1,0,2:T(8,128)(2,1)}), bf16[4,8,8,8,1024]{4,3,1,0,2:T(8,128)(2,1)}) %all-gather.9.cloned.1.call-update) | async-done | bytes 4194320 | tf_op jit(solution)/shard_map/all_gather | solution.py:138
  243.8 7.0 %convert_bitcast_fusion = bf16[4,8,8,8,512]{4,3,1,0,2:T(8,128)(2,1)S(1)} fusion(bf16[4,8,8,8,1024]{4,3,1,0,2:T(8,128)(2,1)} %all-gather.9.cloned.1.call-done, bf16[8,1024,512]{2,1,0:T(8,128)(2,1)} %param.26), kind=kOutput, calls=%fused_computation.14 | convolution fusion | flops 2148532224 | bytes 14680064 | tf_op jit(solution)/shard_map/tsecf,efd->tsecd/dot_general | solution.py:141
  250.8 1.6 copy.69
  252.4 5.6 %all-to-all-start.1 = ((bf16[4,8,8,8,512]{4,3,0,2,1:T(8,128)(2,1)}), bf16[4,8,8,8,512]{4,3,0,2,1:T(8,128)(2,1)S(1)}, u32[]{:S(2)}, u32[]{:S(2)}) async-start(bf16[4,8,8,8,512]{4,3,0,2,1:T(8,128)(2,1)} %copy.69), calls=%async_computation.2 | async-start | bytes 4194304 | tf_op jit(solution)/shard_map/all_to_all | solution.py:147
  258.1 1.6 convert_element_type.61
  259.7 0.7 copy-done.7
  260.4 0.5 fusion.43
  260.8 0.5 fusion.16
  261.3 7.4 %all-gather = bf16[256,1024]{1,0:T(8,128)(2,1)} all-gather(bf16[256,256]{1,0:T(8,128)(2,1)S(1)} %fusion.16), channel_id=2, replica_groups=mesh['sp'=8,'tp'=4] {'tp'}, dimensions={1}, use_global_device_ids=true | all-gather | bytes 655360 | tf_op jit(solution)/shard_map/all_gather | solution.py:139
  268.7 38.0 %all-to-all-done.1 = bf16[4,8,8,8,512]{4,3,0,2,1:T(8,128)(2,1)S(1)} async-done(((bf16[4,8,8,8,512]{4,3,0,2,1:T(8,128)(2,1)}), bf16[4,8,8,8,512]{4,3,0,2,1:T(8,128)(2,1)S(1)}, u32[]{:S(2)}, u32[]{:S(2)}) %all-to-all-start.1) | async-done | bytes 2097184 | tf_op jit(solution)/shard_map/all_to_all | solution.py:147
  306.7 0.3 copy.70
  307.0 0.8 copy-done.6
  307.8 1.2 fusion.42
  308.9 1.1 bitcast_add_fusion
  310.1 1.1 fusion.15
  (60 shorter events, 1.5 us)
Async XLA Ops:
  6.5 13.8 %copy-start = (bf16[256,2048]{1,0:T(8,128)(2,1)S(1)}, bf16[256,2048]{1,0:T(8,128)(2,1)}, u32[]{:S(2)}) copy-start(bf16[256,2048]{1,0:T(8,128)(2,1)} %param.19) | copy-start | bytes 3145732
  6.5 48.2 %reduce-scatter.2.cloned.1.call-start = ((), (), s32[]{:S(2)}) async-start(), calls=%async_computation.3 | async-start | bytes 2621440 | tf_op jit(solution)/shard_map/reduce_scatter | solution.py:99
  6.5 12.9 %copy-start.13 = (f32[4]{0:T(128)S(1)}, f32[4]{0:T(128)}, u32[]{:S(2)}) copy-start(f32[4]{0:T(128)} %param.18) | copy-start | bytes 52
  7.7 8.0 %collective-permute-start = (bf16[128,128]{1,0:T(8,128)(2,1)S(1)}, bf16[128,128]{1,0:T(8,128)(2,1)S(1)}, u32[]{:S(2)}, u32[]{:S(2)}) collective-permute-start(bf16[128,128]{1,0:T(8,128)(2,1)S(1)} %get-tuple-element.10), channel_id=1, source_target_pairs={{0,4},{4,8},{8,12},{12,16},{16,20},{20,24},{24,28},{1,5},{5,9},{9,... | collective-permute-start | bytes 98312 | tf_op jit(solution)/shard_map/ppermute | solution.py:25
  12.6 5.8 %collective-permute-start.1 = (bf16[128,128]{1,0:T(8,128)(2,1)S(1)}, bf16[128,128]{1,0:T(8,128)(2,1)S(1)}, u32[]{:S(2)}, u32[]{:S(2)}) collective-permute-start(bf16[128,128]{1,0:T(8,128)(2,1)S(1)} %get-tuple-element.11), channel_id=1, source_target_pairs={{4,0},{8,4},{12,8},{16,12},{20,16},{24,20},{28,24},{5,1},{9,5},{13... | collective-permute-start | bytes 98312 | tf_op jit(solution)/shard_map/ppermute | solution.py:26
  20.4 34.4 %copy-start.9 = (bf16[64,2048]{1,0:T(8,128)(2,1)S(1)}, bf16[64,2048]{1,0:T(8,128)(2,1)}, u32[]{:S(2)}) copy-start(bf16[64,2048]{1,0:T(8,128)(2,1)} %param.20) | copy-start | bytes 786436
  22.2 34.4 %copy-start.10 = (s32[256,4]{0,1:T(4,128)S(1)}, s32[256,4]{0,1:T(4,128)}, u32[]{:S(2)}) copy-start(s32[256,4]{0,1:T(4,128)} %param.22) | copy-start | bytes 12292
  22.2 38.1 %copy-start.11 = (f32[256,4]{0,1:T(4,128)S(1)}, f32[256,4]{0,1:T(4,128)}, u32[]{:S(2)}) copy-start(f32[256,4]{0,1:T(4,128)} %param.23) | copy-start | bytes 12292
  22.2 38.2 %copy-start.12 = (bf16[2048]{0:T(1024)(128)(2,1)S(1)}, bf16[2048]{0:T(1024)(128)(2,1)}, u32[]{:S(2)}) copy-start(bf16[2048]{0:T(1024)(128)(2,1)} %param.21) | copy-start | bytes 12292
  22.2 51.2 %all-gather.5.cloned.1.call-start = ((), (), s32[]{:S(2)}) async-start(), calls=%async_computation.4 | async-start | bytes 1310720 | tf_op jit(solution)/shard_map/all_gather | solution.py:106
  56.5 132.6 %all-gather.7.cloned.1.call-start = ((), (), s32[]{:S(2)}) async-start(), calls=%async_computation.5 | async-start | bytes 10485760 | tf_op jit(solution)/shard_map/all_gather | solution.py:126
  76.5 54.6 %copy-start.3 = (bf16[256,2048]{1,0:T(8,128)(2,1)}, bf16[256,2048]{1,0:T(8,128)(2,1)S(1)}, u32[]{:S(2)}) copy-start(bf16[256,2048]{1,0:T(8,128)(2,1)S(1)} %multiply_convert_fusion) | copy-start | bytes 3145732
  132.6 111.2 %all-gather.9.cloned.1.call-start = ((), (), s32[]{:S(2)}) async-start(), calls=%async_computation.6 | async-start | bytes 5242880 | tf_op jit(solution)/shard_map/all_gather | solution.py:138
  252.4 5.6 %copy-start.2 = (bf16[256,2048]{1,0:T(8,128)(2,1)S(1)}, bf16[256,2048]{1,0:T(8,128)(2,1)}, u32[]{:S(2)}) copy-start(bf16[256,2048]{1,0:T(8,128)(2,1)} %all-gather.5.cloned.1.call-done) | copy-start | bytes 3145732
  252.4 54.3 %all-to-all-start.1 = ((bf16[4,8,8,8,512]{4,3,0,2,1:T(8,128)(2,1)}), bf16[4,8,8,8,512]{4,3,0,2,1:T(8,128)(2,1)S(1)}, u32[]{:S(2)}, u32[]{:S(2)}) async-start(bf16[4,8,8,8,512]{4,3,0,2,1:T(8,128)(2,1)} %copy.69), calls=%async_computation.2 | async-start | bytes 4194304 | tf_op jit(solution)/shard_map/all_to_all | solution.py:147
  258.1 1.6 copy-start.4
  258.1 2.3 copy-start.7
  258.1 2.8 copy-start.14
  306.7 1.0 copy-start.6
  307.8 2.3 copy-start.5
  307.8 2.3 copy-start.8
  307.8 3.5 %copy-start.1 = (bf16[256,2048]{1,0:T(8,128)(2,1)S(1)}, bf16[256,2048]{1,0:T(8,128)(2,1)}, u32[]{:S(2)}) copy-start(bf16[256,2048]{1,0:T(8,128)(2,1)} %param.19) | copy-start | bytes 3145732
Sparse Core Ops, SparseCore 0:
  22.3 32.3 reduce-scatter.1
  56.7 16.6 all-gather.4
  132.7 56.3 all-gather.6
  208.8 34.9 all-gather.8
where the time goes:
time: 318 us
  waiting for transfers between devices  176 us (55%)
  blocking collectives  61.2 us (19%)
  matrix products  33.1 us (10%)
  between operations  13.5 us (4%)
  other arithmetic  12.7 us (4%)
  starting transfers between devices  12.1 us (4%)
  local copies, waits for them, and re-layouts  8.65 us (3%)
    all_gather x1, waiting for transfers between devices, local(): piece_rows = lax.all_gather(arrived, 'tp', axis=0, tiled=True)  56.3 us
    all_to_all x1, blocking collectives, local(): lax.all_to_all(outgoing, 'sp', split_axis=0, concat_axis=0, tiled=True)  53.9 us
    all_to_all x1, waiting for transfers between devices, local(): lax.all_to_all(routed_total.astype(jnp.bfloat16), 'sp', split_axis=1, con...  38 us
    all_gather x1, waiting for transfers between devices, local(): expert_piece = lax.all_gather(hidden, 'tp', axis=4, tiled=True)  35.2 us
    reduce_scatter x1, waiting for transfers between devices, local(): lax.psum_scatter(jnp.dot(attended, w_out, preferred_element_type=jnp.floa...  32.5 us
    all_gather x1, waiting for transfers between devices, local(): whole_rows = lax.all_gather(mixed_rows, 'tp', axis=0, tiled=True)  11.7 us
    dot_general x1, matrix products, local(): jnp.einsum('tsecd,efd->tsecf', piece_rows, w_up, preferred_element_type=j...  11.4 us
    dot_general x1, matrix products, local(): jnp.einsum('tsecd,efd->tsecf', piece_rows, w_gate, preferred_element_type...  8.13 us
  transfers between devices with their start and end apart: 7, of which 6 were waited for; matrix products, arithmetic and copies ran while one was open for 3% of the time, Pallas kernels for 0%

commit v1 on v0

v1 whole, which is shorter than its diff:
```python
import functools

import jax
import jax.numpy as jnp
from jax import lax
from jax.experimental import pallas as pl
from jax.experimental.pallas import tpu as pltpu
from jax.sharding import PartitionSpec as P

D = 2048
HEADS = 16
KV_HEADS = 4
HD = 64
WINDOW = 128
EXPERTS = 64
TOPK = 4
NORM_EPS = 1e-05
CORES = 2
MOST_BLOCKS = 64
MESH = pl.DeviceIdType.MESH
ANY = pl.BlockSpec(memory_space=pl.ANY)
VMEM = pl.BlockSpec(memory_space=pltpu.VMEM)


def greet(peers):
    barrier = pltpu.get_barrier_semaphore()
    for peer in peers:
        pl.semaphore_signal(barrier, inc=1, device_id=peer, device_id_type=MESH)
    pl.semaphore_wait(barrier, len(peers))


def remote(src, dst, send_sem, recv_sem, peer):
    return pltpu.make_async_remote_copy(
        src_ref=src,
        dst_ref=dst,
        send_sem=send_sem,
        recv_sem=recv_sem,
        device_id=peer,
        device_id_type=MESH,
    )


def grid_of(n_sp, n_tp):
    nx = 1
    while nx * nx * 4 <= n_sp and n_sp % (nx * 2) == 0:
        nx *= 2
    nc = CORES if n_tp % CORES == 0 else 1
    return n_sp // nx, nx, n_tp // nc, nc


def halo_kernel(n_sp, meta_ref, edges_ref, metas_ref, halo_ref, send_sem, recv_sem, edge_send, edge_recv):
    sp, tp = lax.axis_index("sp"), lax.axis_index("tp")
    greet([(lax.rem(sp + d, n_sp), tp) for d in range(1, n_sp)])
    copies = []
    for side, d in ((0, 1), (1, n_sp - 1)):
        copies.append(
            remote(
                edges_ref.at[side],
                halo_ref.at[side],
                edge_send.at[side],
                edge_recv.at[side],
                (lax.rem(sp + d, n_sp), tp),
            )
        )
    for d in range(1, n_sp):
        copies.append(
            remote(
                meta_ref,
                metas_ref.at[d],
                send_sem.at[d - 1],
                recv_sem.at[d - 1],
                (lax.rem(sp + d, n_sp), tp),
            )
        )
    for copy in copies:
        copy.start()
    metas_ref[0] = meta_ref[...]
    for copy in copies:
        copy.wait()


def exchange_halo(meta, edges, n_sp):
    return pl.pallas_call(
        functools.partial(halo_kernel, n_sp),
        out_shape=(
            jax.ShapeDtypeStruct((n_sp,) + meta.shape, meta.dtype),
            jax.ShapeDtypeStruct(edges.shape, edges.dtype),
        ),
        in_specs=[VMEM, VMEM],
        out_specs=(VMEM, VMEM),
        scratch_shapes=[
            pltpu.SemaphoreType.DMA((n_sp - 1,)),
            pltpu.SemaphoreType.DMA((n_sp - 1,)),
            pltpu.SemaphoreType.DMA((2,)),
            pltpu.SemaphoreType.DMA((2,)),
        ],
        compiler_params=pltpu.CompilerParams(collective_id=0, has_side_effects=True),
        name="halo",
    )(meta, edges)


def exchange_kernel(count, pieces, place, parts_ref, out_ref, send_sem, recv_sem):
    me, peer_at = place()
    greet([peer_at(lax.rem(me + d, count)) for d in range(1, count)])
    copies = []
    for piece in range(pieces):
        for d in range(1, count):
            there = lax.rem(me + d, count)
            copies.append(
                remote(
                    parts_ref.at[there, piece],
                    out_ref.at[d - 1, piece],
                    send_sem.at[d - 1, piece],
                    recv_sem.at[d - 1, piece],
                    peer_at(there),
                )
            )
    for copy in copies:
        copy.start()
    for copy in copies:
        copy.wait()


def exchange(parts, count, place, collective_id, name):
    pieces = parts.shape[1]
    return pl.pallas_call(
        functools.partial(exchange_kernel, count, pieces, place),
        out_shape=jax.ShapeDtypeStruct((count - 1,) + parts.shape[1:], parts.dtype),
        in_specs=[ANY],
        out_specs=ANY,
        scratch_shapes=[
            pltpu.SemaphoreType.DMA((count - 1, pieces)),
            pltpu.SemaphoreType.DMA((count - 1, pieces)),
        ],
        compiler_params=pltpu.CompilerParams(
            collective_id=collective_id, has_side_effects=True
        ),
        name=name,
    )(parts)


def world_kernel(grid, own_ref, out_ref, send_sem, recv_sem, own_sem):
    nz, nx, ny, nc = grid
    sp, tp = lax.axis_index("sp"), lax.axis_index("tp")
    z, x, y, c = sp // nx, lax.rem(sp, nx), tp // nc, lax.rem(tp, nc)
    half = own_ref.shape[1] // 2

    def device(dz, dx, dy, dc):
        at_z, at_x = lax.rem(z + dz, nz), lax.rem(x + dx, nx)
        at_y, at_c = lax.rem(y + dy, ny), lax.rem(c + dc, nc)
        return at_z * nx + at_x, at_y * nc + at_c

    z_peers = [device(d, 0, 0, 0) for d in range(1, nz)]
    x_peers = [device(0, d, 0, 0) for d in range(1, nx)]
    y_peers = [device(0, 0, d, 0) for d in range(1, ny)]
    c_peers = [device(0, 0, 0, d) for d in range(1, nc)]
    greet(z_peers + x_peers + y_peers + c_peers)
    sent = []

    def block_of(place):
        at_sp, at_tp = device(*place)
        return at_sp * (ny * nc) + at_tp

    def view(place, h):
        return out_ref.at[block_of(place), :, pl.ds(h * half, half)]

    def push(place, h, peers):
        own = place == (0, 0, 0, 0)
        src = own_ref.at[:, pl.ds(h * half, half)] if own else view(place, h)
        for peer in peers:
            copy = remote(
                src,
                view(place, h),
                send_sem.at[len(sent)],
                recv_sem.at[block_of(place), h],
                peer,
            )
            copy.start()
            sent.append(copy)

    def arrived(place, h):
        remote(
            view(place, h),
            view(place, h),
            send_sem.at[0],
            recv_sem.at[block_of(place), h],
            (sp, tp),
        ).wait_recv()

    mine = (0, 0, 0, 0)
    keep = pltpu.make_async_copy(own_ref, out_ref.at[block_of(mine)], own_sem)
    for h in range(2):
        push(mine, h, z_peers)
    first, second = (x_peers, y_peers), (y_peers, x_peers)
    for h in range(2):
        push(mine, h, first[h])
        push(mine, h, second[h])
        push(mine, h, c_peers)
    keep.start()

    def level_one(dz):
        for h in range(2):
            if dz > 0:
                arrived((dz, 0, 0, 0), h)
                push((dz, 0, 0, 0), h, first[h])
                push((dz, 0, 0, 0), h, second[h])
                push((dz, 0, 0, 0), h, c_peers)

    def level_two(dz):
        for h in range(2):
            for d in range(1, (nx, ny)[h]):
                place = (dz, d, 0, 0) if h == 0 else (dz, 0, d, 0)
                arrived(place, h)
                push(place, h, second[h])
                push(place, h, c_peers)

    def level_three(dz):
        for h in range(2):
            for da in range((nx, ny)[h]):
                for db in range(1, (ny, nx)[h]):
                    place = (dz, da, db, 0) if h == 0 else (dz, db, da, 0)
                    arrived(place, h)
                    push(place, h, c_peers)

    for step in range(nz + 2):
        if step < nz:
            level_one(step)
        if 0 <= step - 1 < nz:
            level_two(step - 1)
        if 0 <= step - 2 < nz:
            level_three(step - 2)
    for dz in range(nz):
        for dx in range(nx):
            for dy in range(ny):
                for dc in range(1, nc):
                    for h in range(2):
                        arrived((dz, dx, dy, dc), h)
    for copy in sent:
        copy.wait_send()
    keep.wait()


def gather_world(own, n_sp, n_tp):
    grid = grid_of(n_sp, n_tp)
    blocks = n_sp * n_tp
    return pl.pallas_call(
        functools.partial(world_kernel, grid),
        out_shape=jax.ShapeDtypeStruct((blocks,) + own.shape, own.dtype),
        in_specs=[VMEM],
        out_specs=ANY,
        scratch_shapes=[
            pltpu.SemaphoreType.DMA((2 * blocks,)),
            pltpu.SemaphoreType.DMA((blocks, 2)),
            pltpu.SemaphoreType.DMA,
        ],
        compiler_params=pltpu.CompilerParams(collective_id=1, has_side_effects=True),
        name="world",
    )(own)


def columns_kernel(ny, nc, pieces, own_ref, out_ref, send_sem, recv_sem, own_sem):
    sp, tp = lax.axis_index("sp"), lax.axis_index("tp")
    y, c = tp // nc, lax.rem(tp, nc)
    rows, width = own_ref.shape
    step = rows // pieces

    def member(dy, dc):
        return lax.rem(y + dy, ny) * nc + lax.rem(c + dc, nc)

    y_peers = [(sp, member(d, 0)) for d in range(1, ny)]
    c_peers = [(sp, member(0, d)) for d in range(1, nc)]
    greet(y_peers + c_peers)
    sent = []

    def view(dy, dc, piece):
        start = pl.multiple_of(member(dy, dc) * width, width)
        return out_ref.at[pl.ds(piece * step, step), pl.ds(start, width)]

    def push(dy, piece, peers):
        src = own_ref.at[pl.ds(piece * step, step)] if dy == 0 else view(dy, 0, piece)
        for peer in peers:
            copy = remote(
                src,
                view(dy, 0, piece),
                send_sem.at[len(sent)],
                recv_sem.at[member(dy, 0), piece],
                peer,
            )
            copy.start()
            sent.append(copy)

    def arrived(dy, dc, piece):
        ref = view(dy, dc, piece)
        remote(
            ref, ref, send_sem.at[0], recv_sem.at[member(dy, dc), piece], (sp, tp)
        ).wait_recv()

    start = pl.multiple_of(tp * width, width)
    keep = pltpu.make_async_copy(own_ref, out_ref.at[:, pl.ds(start, width)], own_sem)
    keep.start()
    for piece in range(pieces):
        push(0, piece, y_peers)
    for piece in range(pieces):
        push(0, piece, c_peers)
    for piece in range(pieces):
        for dy in range(1, ny):
            arrived(dy, 0, piece)
            push(dy, piece, c_peers)
    for piece in range(pieces):
        for dy in range(ny):
            for dc in range(1, nc):
                arrived(dy, dc, piece)
    for copy in sent:
        copy.wait_send()
    keep.wait()


def gather_columns(own, n_sp, n_tp):
    rows, width = own.shape
    if width % 128 or n_sp * n_tp > MOST_BLOCKS:
        return lax.all_gather(own, "tp", axis=1, tiled=True)
    _, _, ny, nc = grid_of(n_sp, n_tp)
    pieces = 9 if rows % (9 * 16) == 0 else 1
    return pl.pallas_call(
        functools.partial(columns_kernel, ny, nc, pieces),
        out_shape=jax.ShapeDtypeStruct((rows, n_tp * width), own.dtype),
        in_specs=[VMEM],
        out_specs=ANY,
        scratch_shapes=[
            pltpu.SemaphoreType.DMA((n_tp * pieces,)),
            pltpu.SemaphoreType.DMA((n_tp, pieces)),
            pltpu.SemaphoreType.DMA,
        ],
        compiler_params=pltpu.CompilerParams(collective_id=2, has_side_effects=True),
        name="columns",
    )(own)


def attention(queries, band, sink, sp_idx, n_sp):
    tok_dev = queries.shape[0]
    blocks = tok_dev // WINDOW
    heads_dev = queries.shape[1] // HD
    framed = band.reshape(blocks + 2, WINDOW, 2 * HD)
    banded = jnp.concatenate([framed[:-2], framed[1:-1], framed[2:]], axis=1)
    key_band = banded[:, :, :HD]
    value_band = banded[:, :, HD:]
    query_blocks = queries.reshape(blocks, WINDOW, heads_dev, HD)
    scores = jnp.einsum(
        "nqhd,njd->nhqj", query_blocks, key_band, preferred_element_type=jnp.float32
    ) * HD ** (-0.5)
    offset = sp_idx * tok_dev
    seq_total = tok_dev * n_sp
    query_pos = (
        offset + jnp.arange(blocks)[:, None, None] * WINDOW + jnp.arange(WINDOW)[None, :, None]
    )
    key_pos = (
        offset
        - WINDOW
        + jnp.arange(blocks)[:, None, None] * WINDOW
        + jnp.arange(3 * WINDOW)[None, None, :]
    )
    allowed = (jnp.abs(query_pos - key_pos) <= WINDOW) & (key_pos >= 0) & (key_pos < seq_total)
    scores = jnp.where(allowed[:, None], scores, -jnp.inf)
    sink_level = sink.reshape(1, heads_dev, 1, 1)
    row_peak = jnp.maximum(scores.max(-1, keepdims=True), sink_level)
    probabilities = jnp.exp(scores - row_peak)
    denominator = probabilities.sum(-1, keepdims=True) + jnp.exp(sink_level - row_peak)
    weights = (probabilities / denominator).astype(jnp.bfloat16)
    attended = jnp.einsum("nhqj,njd->nqhd", weights, value_band, preferred_element_type=jnp.float32)
    return attended.astype(jnp.bfloat16).reshape(tok_dev, heads_dev * HD)


def norm(rows, gain):
    wide = rows.astype(jnp.float32)
    scale = lax.rsqrt(jnp.mean(wide * wide, axis=-1, keepdims=True) + NORM_EPS)
    return (wide * scale * gain.astype(jnp.float32)).astype(jnp.bfloat16)


def local(
    queries,
    keys,
    values,
    sink,
    w_out,
    stream,
    gain,
    routes,
    route_weights,
    w_gate,
    w_up,
    w_down,
    shared_gate,
    shared_up,
    shared_down,
):
    tok_dev = queries.shape[0]
    n_tp = lax.axis_size("tp")
    n_sp = lax.axis_size("sp")
    tp_idx = lax.axis_index("tp")
    sp_idx = lax.axis_index("sp")
    nz, nx, ny, nc = grid_of(n_sp, n_tp)
    z_idx, x_idx = sp_idx // nx, lax.rem(sp_idx, nx)
    heads_dev = HEADS // n_tp
    group = HEADS // KV_HEADS
    kv_head = tp_idx * heads_dev // group
    key_own = lax.dynamic_slice_in_dim(keys, kv_head * HD, HD, 1)
    value_own = lax.dynamic_slice_in_dim(values, kv_head * HD, HD, 1)
    paired = jnp.concatenate([key_own, value_own], axis=1)
    edges = jnp.stack([paired[-WINDOW:], paired[:WINDOW]])
    meta = jnp.concatenate([routes.astype(jnp.float32).T, route_weights.T], axis=0)
    metas, halo = exchange_halo(meta, edges, n_sp)
    band = jnp.concatenate([halo[0], paired, halo[1]], axis=0)
    attended = attention(queries, band, sink, sp_idx, n_sp)
    rows_dev = tok_dev // n_tp
    d_dev = w_down.shape[2]

    partial = jnp.dot(attended, w_out, preferred_element_type=jnp.float32)
    parts = partial.astype(jnp.bfloat16).reshape(n_tp, 1, rows_dev, D)
    theirs = exchange(
        parts,
        n_tp,
        lambda: (lax.axis_index("tp"), lambda there: (lax.axis_index("sp"), there)),
        3,
        "heads",
    )
    own_part = lax.dynamic_slice_in_dim(partial, tp_idx * rows_dev, rows_dev, 0)
    projected = own_part + jnp.sum(theirs[:, 0].astype(jnp.float32), axis=0)
    mixed_rows = (stream.astype(jnp.float32) + projected).astype(jnp.bfloat16)
    if n_sp * n_tp > MOST_BLOCKS:
        normed = lax.all_gather(norm(mixed_rows, gain), ("sp", "tp"), axis=0)
        own_blocks = lax.all_gather(mixed_rows, "tp", axis=0, tiled=True)
    else:
        world = gather_world(mixed_rows, n_sp, n_tp)
        normed = norm(world, gain)
        own_blocks = lax.dynamic_slice_in_dim(world, sp_idx * n_tp, n_tp, 0).reshape(tok_dev, D)
    residual = lax.dynamic_slice_in_dim(own_blocks, tp_idx * d_dev, d_dev, 1).astype(jnp.float32)
    own_normed = norm(own_blocks, gain)

    exp_dev = w_gate.shape[0]
    capacity = max(1, 2 * tok_dev * TOPK // (n_tp * EXPERTS))
    n_blocks = n_sp * n_tp
    order = lax.rem(sp_idx - jnp.arange(n_sp) + n_sp, n_sp)
    pick = (order[None, :] == jnp.arange(n_sp)[:, None]).astype(jnp.float32)
    metas = jnp.sum(pick[:, :, None, None] * metas[None], axis=1)
    metas = metas.reshape(n_sp, 2, TOPK, n_tp, rows_dev).transpose(1, 0, 3, 2, 4)
    named = metas[0].reshape(n_blocks, 1, TOPK, rows_dev)
    weight = metas[1].reshape(n_blocks, 1, TOPK, rows_dev)
    experts = (sp_idx * exp_dev + jnp.arange(exp_dev)).astype(jnp.float32)
    hit = (named == experts[None, :, None, None]).astype(jnp.float32)
    hit_any = jnp.sum(hit, axis=2)
    hit_weight = jnp.sum(hit * weight, axis=2)
    earlier = (jnp.arange(rows_dev)[:, None] < jnp.arange(rows_dev)[None, :]).astype(jnp.bfloat16)
    rank = jnp.einsum(
        "bej,jr->ber", hit_any.astype(jnp.bfloat16), earlier, preferred_element_type=jnp.float32
    )
    slots = jnp.arange(capacity).astype(jnp.float32)
    select = (rank[:, :, None, :] == slots[None, None, :, None]) * hit_any[:, :, None, :]
    slot_weight = jnp.sum(select * hit_weight[:, :, None, :], axis=-1)
    table = select.astype(jnp.bfloat16)

    arrived = jnp.einsum(
        "becr,brd->ebcd", table, normed, preferred_element_type=jnp.float32
    ).astype(jnp.bfloat16)
    arrived = arrived.reshape(exp_dev, n_blocks * capacity, D)
    gate_act = jnp.einsum("emd,efd->emf", arrived, w_gate, preferred_element_type=jnp.float32)
    up_act = jnp.einsum("emd,efd->emf", arrived, w_up, preferred_element_type=jnp.float32)
    hidden = (jax.nn.silu(gate_act) * up_act).astype(jnp.bfloat16)
    shared_gate_act = jnp.einsum(
        "td,fd->tf", own_normed, shared_gate, preferred_element_type=jnp.float32
    )
    shared_up_act = jnp.einsum(
        "td,fd->tf", own_normed, shared_up, preferred_element_type=jnp.float32
    )
    shared_hidden = (jax.nn.silu(shared_gate_act) * shared_up_act).astype(jnp.bfloat16)
    routed_rows = exp_dev * n_blocks * capacity
    width = hidden.shape[2]
    both = jnp.concatenate([hidden.reshape(routed_rows, width), shared_hidden], axis=0)
    both = gather_columns(both, n_sp, n_tp)
    expert_piece = both[:routed_rows].reshape(exp_dev, n_blocks * capacity, n_tp * width)
    routed_out = jnp.einsum(
        "emf,efd->emd", expert_piece, w_down, preferred_element_type=jnp.float32
    )
    scaled = routed_out.reshape(exp_dev, n_blocks, capacity, d_dev)
    scaled = scaled * slot_weight.transpose(1, 0, 2)[..., None]
    scaled = scaled.astype(jnp.bfloat16)
    sums = jnp.einsum("becr,ebcd->brd", table, scaled, preferred_element_type=jnp.float32)
    sums = sums.reshape(nz, nx, tok_dev, d_dev).transpose(1, 0, 2, 3)
    from_x = exchange(
        sums.astype(jnp.bfloat16),
        nx,
        lambda: (
            lax.rem(lax.axis_index("sp"), nx),
            lambda there: (
                lax.axis_index("sp") // nx * nx + there,
                lax.axis_index("tp"),
            ),
        ),
        4,
        "rows_x",
    )
    line = lax.dynamic_index_in_dim(sums, x_idx, 0, keepdims=False)
    line = line + jnp.sum(from_x.astype(jnp.float32), axis=0)
    from_z = exchange(
        line.astype(jnp.bfloat16).reshape(nz, 1, tok_dev, d_dev),
        nz,
        lambda: (
            lax.axis_index("sp") // nx,
            lambda there: (
                there * nx + lax.rem(lax.axis_index("sp"), nx),
                lax.axis_index("tp"),
            ),
        ),
        5,
        "rows_z",
    )
    routed = lax.dynamic_index_in_dim(line, z_idx, 0, keepdims=False)
    routed = routed + jnp.sum(from_z[:, 0].astype(jnp.float32), axis=0)
    shared_total = jnp.dot(both[routed_rows:], shared_down, preferred_element_type=jnp.float32)
    return (residual + routed + shared_total).astype(jnp.bfloat16)


def solution(mesh):
    placed = (
        P("sp", "tp"),
        P("sp", None),
        P("sp", None),
        P("tp"),
        P("tp", None),
        P(("sp", "tp"), None),
        P(),
        P("sp", None),
        P("sp", None),
        P("sp", "tp", None),
        P("sp", "tp", None),
        P("sp", None, "tp"),
        P("tp", None),
        P("tp", None),
        P(None, "tp"),
    )
    return jax.shard_map(
        local, mesh=mesh, in_specs=placed, out_specs=P("sp", "tp"), check_vma=False
    )
```

time: 318 us -> 241 us (0.76)
  waiting for transfers between devices: 176 us -> 0 us
  Pallas kernels: 0 us -> 161 us
  blocking collectives: 61.2 us -> 0 us
  between operations: 13.5 us -> 0.39 us
  starting transfers between devices: 12.1 us -> 0 us
  other arithmetic: 12.7 us -> 23.8 us
  matrix products: 33.1 us -> 43.3 us
    pallas_call x0 -> x6, Pallas kernels: none -> 161 us  [the longest x3 68.2 us: exchange(): pl.pallas_call(functools.partial(exchange_kernel, count, pieces, place),...]
    all_gather x3 -> x0, waiting for transfers between devices: 103 us -> none  [the longest x1 56.3 us: local(): piece_rows = lax.all_gather(arrived, 'tp', axis=0, tiled=True)]
    all_to_all x1 -> x0, blocking collectives: 53.9 us -> none  [local(): lax.all_to_all(outgoing, 'sp', split_axis=0, concat_axis=0, tiled=True)]
    all_to_all x1 -> x0, waiting for transfers between devices: 38 us -> none  [local(): lax.all_to_all(routed_total.astype(jnp.bfloat16), 'sp', split_axis=1, con...]
    reduce_scatter x1 -> x0, waiting for transfers between devices: 32.5 us -> none  [local(): lax.psum_scatter(jnp.dot(attended, w_out, preferred_element_type=jnp.floa...]
    dot_general x11 -> x12, matrix products: 33.1 us -> 43.3 us  [the longest x1 9.67 us: local(): jnp.einsum('emd,efd->emf', arrived, w_gate, preferred_element_type=jnp.fl...]
    reduce_sum x4 -> x9, other arithmetic: 3.16 us -> 11.4 us  [the longest x2 6.65 us: norm(): scale = lax.rsqrt(jnp.mean(wide * wide, axis=-1, keepdims=True) + NORM_EPS)]
    all_gather x1 -> x0, blocking collectives: 7.35 us -> none  [local(): shared_piece = lax.all_gather(shared_hidden, 'tp', axis=4, tiled=True)]
  transfers between devices with their start and end apart: 7 -> 0, of which waited for: 6 -> 0; matrix products, arithmetic and copies ran while one was open for 3% -> 0% of each run, Pallas kernels for 0% -> 0%
where the time goes in v1:
time: 241 us; the launch traced here: 238 us
  Pallas kernels  161 us (67%)
  matrix products  43.3 us (18%)
  other arithmetic  23.8 us (10%)
  local copies, waits for them, and re-layouts  9.11 us (4%)
    pallas_call x3, Pallas kernels, exchange(): pl.pallas_call(functools.partial(exchange_kernel, count, pieces, place),...  68.2 us
    pallas_call x1, Pallas kernels, gather_world(): pl.pallas_call(functools.partial(world_kernel, grid), out_shape=jax.Shape...  50.6 us
    pallas_call x1, Pallas kernels, gather_columns(): pl.pallas_call(functools.partial(columns_kernel, ny, nc, pieces), out_sha...  31.7 us
    pallas_call x1, Pallas kernels, exchange_halo(): pl.pallas_call(functools.partial(halo_kernel, n_sp), out_shape=(jax.Shape...  10.8 us
    dot_general x1, matrix products, local(): jnp.einsum('emd,efd->emf', arrived, w_gate, preferred_element_type=jnp.fl...  9.67 us
    dot_general x1, matrix products, local(): jnp.einsum('becr,brd->ebcd', table, normed, preferred_element_type=jnp.fl...  9.21 us
    dot_general x1, matrix products, local(): jnp.einsum('emd,efd->emf', arrived, w_up, preferred_element_type=jnp.floa...  9.1 us
    reduce_sum x2, other arithmetic, norm(): scale = lax.rsqrt(jnp.mean(wide * wide, axis=-1, keepdims=True) + NORM_EPS)  6.65 us

profile of v1, /device:TPU:0, one launch (start us, length us, event | category | flops | bytes accessed | tf_op | source)
XLA Modules:
  0.0 237.9 jit_solution(15998295649629595335)
XLA Ops:
  0.3 0.7 convert_bitcast_fusion.4
  1.0 1.3 pad_maximum_fusion.8.meta_ref
  2.3 0.7 convert_element_type.129
  3.0 1.1 fusion.37
  4.1 1.0 constant_dynamic-slice_fusion.1
  5.2 0.6 pad_maximum_fusion.6.edges_ref
  5.8 10.8 %halo.1 = (f32[8,8,256]{2,1,0:T(8,128)}, bf16[2,128,128]{2,1,0:T(8,128)(2,1)}) custom-call(f32[8,256]{1,0:T(8,128)} %pad_maximum_fusion.8.meta_ref, bf16[2,128,128]{2,1,0:T(8,128)(2,1)} %pad_maximum_fusion.6.edges_ref), custom_call_target="tpu_custom_call" | custom-call | tf_op jit(solution)/shard_map/halo/pallas_call | solution.py:83
  16.6 0.8 slice_bitcast_fusion.5
  17.5 0.1 copy.41
  17.6 0.1 copy.43
  17.7 1.0 multiply_reduce_fusion.1
  19.0 0.1 copy.42
  19.2 0.2 fusion.30
  19.4 0.1 fusion.43
  19.6 0.4 fusion.28
  20.1 0.2 reshape.247
  20.2 1.1 select_convert_fusion
  21.3 1.3 fusion.58
  22.7 0.2 fusion.24
  23.0 0.4 fusion.27
  23.4 0.1 copy.47
  23.6 1.5 fusion.59
  25.0 13.6 %heads.1 = bf16[3,1,64,2048]{3,2,1,0:T(8,128)(2,1)} custom-call(bf16[4,1,64,2048]{3,2,1,0:T(8,128)(2,1)} %bitcast.105), custom_call_target="tpu_custom_call" | custom-call | tf_op jit(solution)/shard_map/heads/pallas_call | solution.py:126
  38.7 1.3 convert_reduce_fusion.1
  40.0 0.8 add_convert_fusion.own_ref
  40.8 50.6 %world.1 = bf16[32,64,2048]{2,1,0:T(8,128)(2,1)} custom-call(bf16[64,2048]{1,0:T(8,128)(2,1)} %add_convert_fusion.own_ref), custom_call_target="tpu_custom_call" | custom-call | tf_op jit(solution)/shard_map/world/pallas_call | solution.py:246
  91.4 5.1 %fusion = f32[32,64]{1,0:T(8,128)S(1)} fusion(bf16[32,64,2048]{2,1,0:T(8,128)(2,1)} %world.1), kind=kLoop, calls=%fused_computation.2 | loop fusion | flops 12580864 | bytes 8396800 | tf_op jit(solution)/shard_map/reduce_sum | solution.py:375
  96.5 1.6 multiply_reduce_fusion
  98.1 9.2 %convert_bitcast_fusion = bf16[8,32,8,2048]{3,2,0,1:T(8,128)(2,1)} fusion(bf16[32,64,2048]{2,1,0:T(8,128)(2,1)} %world.1, f32[2048]{0:T(1024)S(1)} %convert_element_type.129, f32[32,64]{1,0:T(8,128)S(1)} %add_rsqrt_fusion, bf16[32,8,8,64]{3,1,2,0:T(8,128)(2,1)S(1)} %copy-done.5), kind=kOutput, calls=%fused_computation.11 | convolution fusion | flops 557842432 | bytes 17055744 | tf_op jit(solution)/shard_map/becr,brd->ebcd/dot_general | solution.py:461
  107.4 0.5 fusion.38
  107.9 0.7 copy-done.10
  108.6 0.5 fusion.26
  109.1 9.7 %fusion.8 = f32[8,256,256]{2,1,0:T(8,128)} fusion(bf16[8,256,2048]{2,1,0:T(8,128)(2,1)} %param.24, bf16[8,32,8,2048]{3,2,0,1:T(8,128)(2,1)} %convert_bitcast_fusion), kind=kOutput, calls=%fused_computation.9 | convolution fusion | flops 2147483648 | bytes 18874368 | tf_op jit(solution)/shard_map/emd,efd->emf/dot_general | solution.py:465
  118.8 9.1 %multiply_convert_fusion.1 = bf16[8,256,256]{2,1,0:T(8,128)(2,1)S(1)} fusion(f32[8,256,256]{2,1,0:T(8,128)} %fusion.8, bf16[8,256,2048]{2,1,0:T(8,128)(2,1)} %param.25, bf16[8,32,8,2048]{3,2,0,1:T(8,128)(2,1)} %convert_bitcast_fusion), kind=kOutput, calls=%fused_computation.28 | convolution fusion | flops 2150629376 | bytes 19922944 | tf_op jit(solution)/shard_map/emd,efd->emf/dot_general | solution.py:466
  127.9 1.1 pad_maximum_fusion.own_ref
  129.0 31.7 %columns.1 = bf16[2304,1024]{1,0:T(8,128)(2,1)} custom-call(bf16[2304,256]{1,0:T(8,128)(2,1)} %pad_maximum_fusion.own_ref), custom_call_target="tpu_custom_call" | custom-call | tf_op jit(solution)/shard_map/columns/pallas_call | solution.py:324
  160.7 2.2 slice-done
  162.9 5.7 %convolution_bitcast_fusion = f32[8,32,8,512]{3,2,1,0:T(8,128)S(1)} fusion(bf16[8,256,1024]{2,1,0:T(8,128)(2,1)S(1)} %bitcast.104, bf16[8,1024,512]{2,1,0:T(8,128)(2,1)} %param.26), kind=kOutput, calls=%fused_computation.20 | convolution fusion | flops 2147483648 | bytes 16777216 | tf_op jit(solution)/shard_map/emf,efd->emd/dot_general | solution.py:480
  168.6 3.0 %fusion.19 = f32[32,64,512,1]{2,1,3,0:T(8,128)S(1)} fusion(f32[8,32,8,512]{3,2,1,0:T(8,128)S(1)} %convolution_bitcast_fusion, f32[8,32,8]{0,2,1:T(8,128)S(1)} %bitcast.110, f32[32,8,64]{2,1,0:T(8,128)S(1)} %get-tuple-element.10, f32[32,8,64]{2,1,0:T(8,128)S(1)} %copy.51, f32[8]{0:T(128)S(1)} %iota_convert_fusion), kind=kOutput, calls=%fused_computation.23 | convolution fusion | flops 136577024 | bytes 8527904 | tf_op jit(solution)/shard_map/becr,ebcd->brd/dot_general | solution.py:486
  171.6 0.3 convert_bitcast_fusion.3
  171.9 1.7 copy-done.2
  173.6 1.6 copy.56.parts_ref
  175.2 25.9 %rows_x.1 = bf16[1,4,256,512]{3,2,1,0:T(8,128)(2,1)} custom-call(bf16[2,4,256,512]{3,2,1,0:T(8,128)(2,1)} %copy.56.parts_ref), custom_call_target="tpu_custom_call" | custom-call | tf_op jit(solution)/shard_map/rows_x/pallas_call | solution.py:126
  201.1 4.0 %dynamic-slice_bitcast_fusion = (f32[4,256,512]{2,1,0:T(8,128)}, bf16[4,1,256,512]{3,2,1,0:T(8,128)(2,1)}) fusion(f32[4,2,256,512]{3,2,1,0:T(8,128)} %bitcast.103, s32[]{:T(128)S(6)} %select_n.39, bf16[1,4,256,512]{3,2,1,0:T(8,128)(2,1)} %rows_x.1), kind=kLoop, calls=%fused_computation.29 | loop fusion | flops 1572864 | bytes 6291460 | tf_op jit(solution)/shard_map/jit(dynamic_index_in_dim)/squeeze | solution.py:501
  205.1 28.7 %rows_z.1 = bf16[3,1,256,512]{3,2,1,0:T(8,128)(2,1)} custom-call(bf16[4,1,256,512]{3,2,1,0:T(8,128)(2,1)} %get-tuple-element.14.parts_ref), custom_call_target="tpu_custom_call" | custom-call | tf_op jit(solution)/shard_map/rows_z/pallas_call | solution.py:126
  233.9 1.4 convert_reduce_fusion
  235.3 0.3 convert_bitcast_fusion.2
  235.6 2.4 fusion.25
  (45 shorter events, 1.1 us)
Async XLA Ops:
  0.0 23.6 %copy-start = (bf16[256,2048]{1,0:T(8,128)(2,1)S(1)}, bf16[256,2048]{1,0:T(8,128)(2,1)}, u32[]{:S(2)}) copy-start(bf16[256,2048]{1,0:T(8,128)(2,1)} %param.19) | copy-start | bytes 3145732
  5.1 14.9 %copy-start.7 = (bf16[256,256]{1,0:T(8,128)(2,1)S(1)}, bf16[256,256]{1,0:T(8,128)(2,1)}, u32[]{:S(2)}) copy-start(bf16[256,256]{1,0:T(8,128)(2,1)} %param.15) | copy-start | bytes 393220
  19.4 3.2 %copy-start.8 = (f32[4]{0:T(128)S(1)}, f32[4]{0:T(128)}, u32[]{:S(2)}) copy-start(f32[4]{0:T(128)} %param.18) | copy-start | bytes 52
  25.0 15.0 %copy-start.6 = (bf16[64,2048]{1,0:T(8,128)(2,1)S(1)}, bf16[64,2048]{1,0:T(8,128)(2,1)}, u32[]{:S(2)}) copy-start(bf16[64,2048]{1,0:T(8,128)(2,1)} %param.20) | copy-start | bytes 786436
  96.5 1.6 copy-start.5
  98.1 9.3 %copy-start.9 = (bf16[256,2048]{1,0:T(8,128)(2,1)S(1)}, bf16[256,2048]{1,0:T(8,128)(2,1)}, u32[]{:S(2)}) copy-start(bf16[256,2048]{1,0:T(8,128)(2,1)} %param.27) | copy-start | bytes 3145732
  107.4 1.2 copy-start.10
  160.7 2.2 slice-start
  171.6 2.0 copy-start.2
  205.1 30.1 %copy-start.3 = (bf16[1,4,256,512]{3,2,1,0:T(8,128)(2,1)S(1)}, bf16[1,4,256,512]{3,2,1,0:T(8,128)(2,1)}, u32[]{:S(2)}) copy-start(bf16[1,4,256,512]{3,2,1,0:T(8,128)(2,1)} %rows_x.1) | copy-start | bytes 3145732
  233.9 1.7 copy-start.4
  235.3 2.7 %copy-start.1 = (bf16[256,2048]{1,0:T(8,128)(2,1)S(1)}, bf16[256,2048]{1,0:T(8,128)(2,1)}, u32[]{:S(2)}) copy-start(bf16[256,2048]{1,0:T(8,128)(2,1)} %param.19) | copy-start | bytes 3145732

commit v2 on v1

--- a/solution.py
+++ b/solution.py
@@ -189,8 +189,9 @@
 
     mine = (0, 0, 0, 0)
     keep = pltpu.make_async_copy(own_ref, out_ref.at[block_of(mine)], own_sem)
-    for h in range(2):
-        push(mine, h, z_peers)
+    for peer in z_peers:
+        for h in range(2):
+            push(mine, h, [peer])
     first, second = (x_peers, y_peers), (y_peers, x_peers)
     for h in range(2):
         push(mine, h, first[h])
@@ -222,13 +223,12 @@
                     arrived(place, h)
                     push(place, h, c_peers)
 
-    for step in range(nz + 2):
+    for step in range(nz + 1):
         if step < nz:
             level_one(step)
-        if 0 <= step - 1 < nz:
-            level_two(step - 1)
-        if 0 <= step - 2 < nz:
-            level_three(step - 2)
+            level_two(step)
+        if step > 0:
+            level_three(step - 1)
     for dz in range(nz):
         for dx in range(nx):
             for dy in range(ny):
@@ -334,6 +334,95 @@
         compiler_params=pltpu.CompilerParams(collective_id=2, has_side_effects=True),
         name="columns",
     )(own)
+
+
+def rows_kernel(grid, cuts, parts_ref, columns_ref, own_ref, from_z_ref, residual_ref, from_x, staged, x_send, x_recv, z_send, z_recv, tp_send, tp_recv):
+    nz, nx, ny, nc = grid
+    n_tp = ny * nc
+    sp, tp = lax.axis_index("sp"), lax.axis_index("tp")
+    z, x = sp // nx, lax.rem(sp, nx)
+    x_peers = [(z * nx + lax.rem(x + d, nx), tp) for d in range(1, nx)]
+    z_peers = [(lax.rem(z + d, nz) * nx + x, tp) for d in range(1, nz)]
+    tp_peers = [(sp, lax.rem(tp + d, n_tp)) for d in range(1, n_tp)]
+    greet(x_peers + z_peers + tp_peers)
+    step = parts_ref.shape[2] // cuts
+    turns = [(dz, cut) for dz in list(range(1, nz)) + [0] for cut in range(cuts)]
+    x_copies, others = {}, []
+    for dz, cut in turns:
+        rows = pl.ds(cut * step, step)
+        for d in range(1, nx):
+            copy = remote(
+                parts_ref.at[lax.rem(z + dz, nz), lax.rem(x + d, nx), rows],
+                from_x.at[d - 1, dz, rows],
+                x_send.at[d - 1, dz, cut],
+                x_recv.at[d - 1, dz, cut],
+                x_peers[d - 1],
+            )
+            copy.start()
+            x_copies[d, dz, cut] = copy
+    for d in range(1, n_tp):
+        copy = remote(
+            columns_ref.at[lax.rem(tp + d, n_tp)],
+            residual_ref.at[tp],
+            tp_send.at[d - 1],
+            tp_recv.at[d - 1],
+            tp_peers[d - 1],
+        )
+        copy.start()
+        others.append(copy)
+    residual_ref[tp] = columns_ref[tp]
+    for dz, cut in turns:
+        rows = pl.ds(cut * step, step)
+        total = parts_ref[lax.rem(z + dz, nz), x, rows].astype(jnp.float32)
+        for d in range(1, nx):
+            x_copies[d, dz, cut].wait_recv()
+            total = total + from_x[d - 1, dz, rows].astype(jnp.float32)
+        if dz == 0:
+            own_ref[rows] = total
+            continue
+        staged[dz - 1, rows] = total.astype(staged.dtype)
+        copy = remote(
+            staged.at[dz - 1, rows],
+            from_z_ref.at[dz - 1, rows],
+            z_send.at[dz - 1, cut],
+            z_recv.at[dz - 1, cut],
+            z_peers[dz - 1],
+        )
+        copy.start()
+        others.append(copy)
+    for copy in x_copies.values():
+        copy.wait_send()
+    for copy in others:
+        copy.wait()
+
+
+def sum_rows(parts, columns, n_sp, n_tp):
+    grid = grid_of(n_sp, n_tp)
+    nz, nx, _, _ = grid
+    tok_dev, d_dev = parts.shape[2:]
+    cuts = 2
+    return pl.pallas_call(
+        functools.partial(rows_kernel, grid, cuts),
+        out_shape=(
+            jax.ShapeDtypeStruct((tok_dev, d_dev), jnp.float32),
+            jax.ShapeDtypeStruct((nz - 1, tok_dev, d_dev), parts.dtype),
+            jax.ShapeDtypeStruct(columns.shape, columns.dtype),
+        ),
+        in_specs=[VMEM, VMEM],
+        out_specs=(VMEM, VMEM, VMEM),
+        scratch_shapes=[
+            pltpu.VMEM((nx - 1, nz, tok_dev, d_dev), parts.dtype),
+            pltpu.VMEM((nz - 1, tok_dev, d_dev), parts.dtype),
+            pltpu.SemaphoreType.DMA((nx - 1, nz, cuts)),
+            pltpu.SemaphoreType.DMA((nx - 1, nz, cuts)),
+            pltpu.SemaphoreType.DMA((nz - 1, cuts)),
+            pltpu.SemaphoreType.DMA((nz - 1, cuts)),
+            pltpu.SemaphoreType.DMA((n_tp - 1,)),
+            pltpu.SemaphoreType.DMA((n_tp - 1,)),
+        ],
+        compiler_params=pltpu.CompilerParams(collective_id=4, has_side_effects=True),
+        name="rows",
+    )(parts, columns)
 
 
 def attention(queries, band, sink, sp_idx, n_sp):
@@ -398,8 +487,7 @@
     n_sp = lax.axis_size("sp")
     tp_idx = lax.axis_index("tp")
     sp_idx = lax.axis_index("sp")
-    nz, nx, ny, nc = grid_of(n_sp, n_tp)
-    z_idx, x_idx = sp_idx // nx, lax.rem(sp_idx, nx)
+    nz, nx, _, _ = grid_of(n_sp, n_tp)
     heads_dev = HEADS // n_tp
     group = HEADS // KV_HEADS
     kv_head = tp_idx * heads_dev // group
@@ -426,15 +514,12 @@
     own_part = lax.dynamic_slice_in_dim(partial, tp_idx * rows_dev, rows_dev, 0)
     projected = own_part + jnp.sum(theirs[:, 0].astype(jnp.float32), axis=0)
     mixed_rows = (stream.astype(jnp.float32) + projected).astype(jnp.bfloat16)
+    own_norm = norm(mixed_rows, gain)
     if n_sp * n_tp > MOST_BLOCKS:
-        normed = lax.all_gather(norm(mixed_rows, gain), ("sp", "tp"), axis=0)
-        own_blocks = lax.all_gather(mixed_rows, "tp", axis=0, tiled=True)
+        normed = lax.all_gather(own_norm, ("sp", "tp"), axis=0)
     else:
-        world = gather_world(mixed_rows, n_sp, n_tp)
-        normed = norm(world, gain)
-        own_blocks = lax.dynamic_slice_in_dim(world, sp_idx * n_tp, n_tp, 0).reshape(tok_dev, D)
-    residual = lax.dynamic_slice_in_dim(own_blocks, tp_idx * d_dev, d_dev, 1).astype(jnp.float32)
-    own_normed = norm(own_blocks, gain)
+        normed = gather_world(own_norm, n_sp, n_tp)
+    own_normed = lax.dynamic_slice_in_dim(normed, sp_idx * n_tp, n_tp, 0).reshape(tok_dev, D)
 
     exp_dev = w_gate.shape[0]
     capacity = max(1, 2 * tok_dev * TOPK // (n_tp * EXPERTS))
@@ -484,37 +569,11 @@
     scaled = scaled * slot_weight.transpose(1, 0, 2)[..., None]
     scaled = scaled.astype(jnp.bfloat16)
     sums = jnp.einsum("becr,ebcd->brd", table, scaled, preferred_element_type=jnp.float32)
-    sums = sums.reshape(nz, nx, tok_dev, d_dev).transpose(1, 0, 2, 3)
-    from_x = exchange(
-        sums.astype(jnp.bfloat16),
-        nx,
-        lambda: (
-            lax.rem(lax.axis_index("sp"), nx),
-            lambda there: (
-                lax.axis_index("sp") // nx * nx + there,
-                lax.axis_index("tp"),
-            ),
-        ),
-        4,
-        "rows_x",
-    )
-    line = lax.dynamic_index_in_dim(sums, x_idx, 0, keepdims=False)
-    line = line + jnp.sum(from_x.astype(jnp.float32), axis=0)
-    from_z = exchange(
-        line.astype(jnp.bfloat16).reshape(nz, 1, tok_dev, d_dev),
-        nz,
-        lambda: (
-            lax.axis_index("sp") // nx,
-            lambda there: (
-                there * nx + lax.rem(lax.axis_index("sp"), nx),
-                lax.axis_index("tp"),
-            ),
-        ),
-        5,
-        "rows_z",
-    )
-    routed = lax.dynamic_index_in_dim(line, z_idx, 0, keepdims=False)
-    routed = routed + jnp.sum(from_z[:, 0].astype(jnp.float32), axis=0)
+    sums = sums.astype(jnp.bfloat16).reshape(nz, nx, tok_dev, d_dev)
+    columns = mixed_rows.reshape(rows_dev, n_tp, d_dev).transpose(1, 0, 2)
+    own_sum, from_z, residual = sum_rows(sums, columns, n_sp, n_tp)
+    residual = residual.reshape(tok_dev, d_dev).astype(jnp.float32)
+    routed = own_sum + jnp.sum(from_z.astype(jnp.float32), axis=0)
     shared_total = jnp.dot(both[routed_rows:], shared_down, preferred_element_type=jnp.float32)
     return (residual + routed + shared_total).astype(jnp.bfloat16)
 

time: 241 us -> 212 us (0.88)
  other arithmetic: 23.8 us -> 9.87 us
  Pallas kernels: 161 us -> 148 us
    pallas_call x3 -> x1, Pallas kernels: 68.2 us -> 13.6 us  [exchange(): pl.pallas_call(functools.partial(exchange_kernel, count, pieces, place),...]
    pallas_call x0 -> x1, Pallas kernels: none -> 43 us  [sum_rows(): pl.pallas_call(functools.partial(rows_kernel, grid, cuts), out_shape=(jax...]
    reduce_sum x2 -> x1, other arithmetic: 6.65 us -> 0.2 us  [norm(): scale = lax.rsqrt(jnp.mean(wide * wide, axis=-1, keepdims=True) + NORM_EPS)]
    squeeze x1 -> x0, other arithmetic: 4.01 us -> none  [local(): line = lax.dynamic_index_in_dim(sums, x_idx, 0, keepdims=False)]
    unnamed x22 -> x16, local copies, waits for them, and re-layouts: 2.51 us -> 0.03 us
where the time goes in v2:
time: 212 us; the launch traced here: 211 us
  Pallas kernels  148 us (70%)
  matrix products  44.5 us (21%)
  other arithmetic  9.87 us (5%)
  local copies, waits for them, and re-layouts  8.02 us (4%)
    pallas_call x1, Pallas kernels, gather_world(): pl.pallas_call(functools.partial(world_kernel, grid), out_shape=jax.Shape...  49.1 us
    pallas_call x1, Pallas kernels, sum_rows(): pl.pallas_call(functools.partial(rows_kernel, grid, cuts), out_shape=(jax...  43 us
    pallas_call x1, Pallas kernels, gather_columns(): pl.pallas_call(functools.partial(columns_kernel, ny, nc, pieces), out_sha...  31.7 us
    pallas_call x1, Pallas kernels, exchange(): pl.pallas_call(functools.partial(exchange_kernel, count, pieces, place),...  13.6 us
    pallas_call x1, Pallas kernels, exchange_halo(): pl.pallas_call(functools.partial(halo_kernel, n_sp), out_shape=(jax.Shape...  10.8 us
    dot_general x1, matrix products, local(): jnp.einsum('emd,efd->emf', arrived, w_gate, preferred_element_type=jnp.fl...  9.48 us
    dot_general x1, matrix products, local(): jnp.einsum('emd,efd->emf', arrived, w_up, preferred_element_type=jnp.floa...  9.09 us
    dot_general x1, matrix products, local(): jnp.einsum('becr,brd->ebcd', table, normed, preferred_element_type=jnp.fl...  8.91 us

profile of v2, /device:TPU:0, one launch (start us, length us, event | category | flops | bytes accessed | tf_op | source)
XLA Modules:
  0.0 211.1 jit_solution(216125418920448806)
XLA Ops:
  0.0 1.2 reshape.229
  1.2 0.7 convert_bitcast_fusion.1
  1.9 1.3 pad_maximum_fusion.8.meta_ref
  3.2 1.0 constant_dynamic-slice_fusion.1
  4.1 0.1 fusion.36
  4.2 0.6 pad_maximum_fusion.6.edges_ref
  4.9 10.8 %halo.1 = (f32[8,8,256]{2,1,0:T(8,128)}, bf16[2,128,128]{2,1,0:T(8,128)(2,1)}) custom-call(f32[8,256]{1,0:T(8,128)} %pad_maximum_fusion.8.meta_ref, bf16[2,128,128]{2,1,0:T(8,128)(2,1)} %pad_maximum_fusion.6.edges_ref), custom_call_target="tpu_custom_call" | custom-call | tf_op jit(solution)/shard_map/halo/pallas_call | solution.py:83
  15.7 0.8 slice_bitcast_fusion.5
  16.5 0.1 pad_maximum_fusion.4
  16.6 0.1 copy.46
  16.7 0.1 copy.45
  16.8 0.1 copy.44
  17.1 0.1 iota_add_fusion.1
  17.2 0.1 fusion.43
  17.2 0.5 fusion.28
  17.7 0.4 fusion.48
  18.2 0.2 fusion.15
  18.5 0.1 exponential_add_fusion
  18.6 0.4 fusion.18
  19.0 0.1 copy.50
  19.1 1.5 fusion.49
  20.6 13.6 %heads.1 = bf16[3,1,64,2048]{3,2,1,0:T(8,128)(2,1)} custom-call(bf16[4,1,64,2048]{3,2,1,0:T(8,128)(2,1)} %bitcast.97), custom_call_target="tpu_custom_call" | custom-call | tf_op jit(solution)/shard_map/heads/pallas_call | solution.py:126
  34.2 1.3 convert_reduce_fusion.1
  35.5 0.2 fusion.20
  35.8 0.8 fusion.22.own_ref
  36.6 49.1 %world.1 = bf16[32,64,2048]{2,1,0:T(8,128)(2,1)} custom-call(bf16[64,2048]{1,0:T(8,128)(2,1)} %fusion.22.own_ref), custom_call_target="tpu_custom_call" | custom-call | tf_op jit(solution)/shard_map/world/pallas_call | solution.py:246
  85.7 1.3 constant_dynamic-slice_fusion
  87.1 0.5 fusion.50
  87.6 1.7 fusion.17
  89.3 0.1 multiply_reduce_fusion
  89.5 0.1 reshape.212
  89.7 0.2 fusion.24
  90.0 0.1 fusion.33
  90.1 0.1 copy.43
  90.2 0.2 select_convert_fusion
  90.4 8.9 %convert_bitcast_fusion = bf16[8,32,8,2048]{3,2,0,1:T(8,128)(2,1)} fusion(bf16[32,64,2048]{2,1,0:T(8,128)(2,1)} %world.1, bf16[32,8,8,64]{3,1,2,0:T(8,128)(2,1)S(1)} %select_convert_fusion), kind=kOutput, calls=%fused_computation.6 | convolution fusion | flops 541065216 | bytes 17039360 | tf_op jit(solution)/shard_map/becr,brd->ebcd/dot_general | solution.py:546
  99.3 9.5 %fusion.4 = f32[8,256,256]{2,1,0:T(8,128)} fusion(bf16[8,256,2048]{2,1,0:T(8,128)(2,1)} %param.24, bf16[8,32,8,2048]{3,2,0,1:T(8,128)(2,1)} %convert_bitcast_fusion), kind=kOutput, calls=%fused_computation.4 | convolution fusion | flops 2147483648 | bytes 18874368 | tf_op jit(solution)/shard_map/emd,efd->emf/dot_general | solution.py:550
  108.8 9.1 %multiply_convert_fusion = bf16[8,256,256]{2,1,0:T(8,128)(2,1)S(1)} fusion(f32[8,256,256]{2,1,0:T(8,128)} %fusion.4, bf16[8,256,2048]{2,1,0:T(8,128)(2,1)} %param.25, bf16[8,32,8,2048]{3,2,0,1:T(8,128)(2,1)} %convert_bitcast_fusion), kind=kOutput, calls=%fused_computation.14 | convolution fusion | flops 2150629376 | bytes 19922944 | tf_op jit(solution)/shard_map/emd,efd->emf/dot_general | solution.py:551
  117.9 1.3 pad_maximum_fusion.own_ref
  119.2 31.7 %columns.1 = bf16[2304,1024]{1,0:T(8,128)(2,1)} custom-call(bf16[2304,256]{1,0:T(8,128)(2,1)} %pad_maximum_fusion.own_ref), custom_call_target="tpu_custom_call" | custom-call | tf_op jit(solution)/shard_map/columns/pallas_call | solution.py:324
  150.9 2.2 %slice-done = bf16[2048,1024]{1,0:T(8,128)(2,1)S(1)} async-done(((bf16[2304,1024]{1,0:T(8,128)(2,1)}), bf16[2048,1024]{1,0:T(8,128)(2,1)S(1)}, s32[]{:S(2)}) %slice-start) | async-done | bytes 4194328 | tf_op jit(solution)/shard_map/slice | solution.py:564
  153.1 5.7 %convolution_bitcast_fusion = f32[8,32,8,512]{3,2,1,0:T(8,128)S(1)} fusion(bf16[8,256,1024]{2,1,0:T(8,128)(2,1)S(1)} %bitcast.93, bf16[8,1024,512]{2,1,0:T(8,128)(2,1)} %param.26), kind=kOutput, calls=%fused_computation.12 | convolution fusion | flops 2147483648 | bytes 16777216 | tf_op jit(solution)/shard_map/emf,efd->emd/dot_general | solution.py:565
  158.8 0.4 fusion.19
  159.2 4.3 %bitcast_convert_fusion = bf16[32,64,512]{2,1,0:T(8,128)(2,1)} fusion(f32[8,32,8,512]{3,2,1,0:T(8,128)S(1)} %convolution_bitcast_fusion, f32[8,32,8]{0,2,1:T(8,128)S(1)} %bitcast.101, f32[32,8,64]{2,1,0:T(8,128)S(1)} %get-tuple-element.16, f32[32,8,64]{2,1,0:T(8,128)S(1)} %copy.43, f32[8]{0:T(128)S(1)} %iota_convert_fusion), kind=kOutput, calls=%fused_computation.9 | convolution fusion | flops 137625600 | bytes 6430752 | tf_op jit(solution)/shard_map/becr,ebcd->brd/dot_general | solution.py:571
  163.6 0.7 copy.95
  164.3 43.0 %rows.1 = (f32[256,512]{1,0:T(8,128)}, bf16[3,256,512]{2,1,0:T(8,128)(2,1)}, bf16[4,64,512]{2,1,0:T(8,128)(2,1)}) custom-call(bf16[4,2,256,512]{3,2,1,0:T(8,128)(2,1)} %bitcast.94, bf16[4,64,512]{2,1,0:T(8,128)(2,1)} %bitcast.99), custom_call_target="tpu_custom_call" | custom-call | tf_op jit(solution)/shard_map/rows/pallas_call | solution.py:404
  207.4 1.3 convert_reduce_fusion
  208.7 2.4 %fusion.16 = bf16[256,512]{1,0:T(8,128)(2,1)} fusion(bf16[1024,512]{1,0:T(8,128)(2,1)S(1)} %copy-done.2, bf16[256,512]{1,0:T(8,128)(2,1)} %bitcast.104, bf16[2304,1024]{1,0:T(8,128)(2,1)} %columns.1, f32[256,512]{1,0:T(8,128)} %get-tuple-element.13, f32[256,512]{1,0:T(8,128)S(1)} %convert_reduce_fusion), kind=kOutput, calls=%fused_computation.24 | convolution fusion | flops 269090816 | bytes 3145728 | tf_op jit(solution)/shard_map/dot_general | solution.py:577
  (33 shorter events, 0.4 us)
Async XLA Ops:
  0.0 19.1 %copy-start = (bf16[256,2048]{1,0:T(8,128)(2,1)S(1)}, bf16[256,2048]{1,0:T(8,128)(2,1)}, u32[]{:S(2)}) copy-start(bf16[256,2048]{1,0:T(8,128)(2,1)} %param.19) | copy-start | bytes 3145732
  0.0 18.2 %copy-start.7 = (f32[4]{0:T(128)S(1)}, f32[4]{0:T(128)}, u32[]{:S(2)}) copy-start(f32[4]{0:T(128)} %param.18) | copy-start | bytes 52
  20.6 15.0 %copy-start.4 = (bf16[64,2048]{1,0:T(8,128)(2,1)S(1)}, bf16[64,2048]{1,0:T(8,128)(2,1)}, u32[]{:S(2)}) copy-start(bf16[64,2048]{1,0:T(8,128)(2,1)} %param.20) | copy-start | bytes 786436
  20.6 15.2 %copy-start.6 = (bf16[2048]{0:T(1024)(128)(2,1)S(1)}, bf16[2048]{0:T(1024)(128)(2,1)}, u32[]{:S(2)}) copy-start(bf16[2048]{0:T(1024)(128)(2,1)} %param.21) | copy-start | bytes 12292
  36.6 50.5 %copy-start.3 = (bf16[256,2048]{1,0:T(8,128)(2,1)S(1)}, bf16[256,2048]{1,0:T(8,128)(2,1)}, u32[]{:S(2)}) copy-start(bf16[256,2048]{1,0:T(8,128)(2,1)} %param.27) | copy-start | bytes 3145732
  87.1 2.2 %copy-start.5 = (f32[8,8,256]{2,1,0:T(8,128)S(1)}, f32[8,8,256]{2,1,0:T(8,128)}, u32[]{:S(2)}) copy-start(f32[8,8,256]{2,1,0:T(8,128)} %get-tuple-element.10) | copy-start | bytes 196612
  150.9 2.2 %slice-start = ((bf16[2304,1024]{1,0:T(8,128)(2,1)}), bf16[2048,1024]{1,0:T(8,128)(2,1)S(1)}, s32[]{:S(2)}) async-start(bf16[2304,1024]{1,0:T(8,128)(2,1)} %columns.1), calls=%async_computation | async-start | bytes 8388608 | tf_op jit(solution)/shard_map/slice | solution.py:564
  163.6 45.1 %copy-start.2 = (bf16[1024,512]{1,0:T(8,128)(2,1)S(1)}, bf16[1024,512]{1,0:T(8,128)(2,1)}, u32[]{:S(2)}) copy-start(bf16[1024,512]{1,0:T(8,128)(2,1)} %param.29) | copy-start | bytes 3145732
  164.3 46.8 %copy-start.1 = (bf16[256,2048]{1,0:T(8,128)(2,1)S(1)}, bf16[256,2048]{1,0:T(8,128)(2,1)}, u32[]{:S(2)}) copy-start(bf16[256,2048]{1,0:T(8,128)(2,1)} %param.19) | copy-start | bytes 3145732
